TPU v7x, 512 devices: a 4x2x32 block of a 4x8x32 slice. The times are simulated.
512 devices in a mesh: grp: 2 (over y), sp: 32 (over z), tp: 8 (over x, core).
Axes of the slice: x: 4, y: 2, z: 32, core: 2. Of those that a mesh axis runs over, the one named last changes fastest.
The devices are a block of a 4x8x32 slice.
Arguments:
- tokens: bfloat16 [2048, 8, 2048], P(('sp', 'tp'), 'grp'), parts along dimension 1, may hold values from -6 to 6
- norm_gain: float32 [2048], replicated, may hold values from 0.1 to 1.9
- w_query: bfloat16 [2048, 2048], P('sp', 'tp'), may hold values from -0.125 to 0.125
- w_value: bfloat16 [2048, 2048], P('sp', 'tp'), may hold values from -0.125 to 0.125
- w_fwd_gate: bfloat16 [2048, 2048], P('sp', 'tp'), may hold values from -0.125 to 0.125
- w_bwd_gate: bfloat16 [2048, 2048], P('sp', 'tp'), may hold values from -0.125 to 0.125
- w_out_gate: bfloat16 [2048, 2048], P('sp', 'tp'), may hold values from -0.125 to 0.125
- floor_gap: float32 [2, 2048], P(None, 'tp'), may hold values from 9.765625e-05 to 0.1
- decay_shift: float32 [2048, 8, 2048], P('sp', 'grp', 'tp'), parts along dimension 1, may hold values from -1.1 to 0
- head_gain: float32 [128], replicated, may hold values from 0.1 to 1.9
- w_out: bfloat16 [2048, 2048], P('tp', 'sp'), may hold values from -0.125 to 0.125
Outputs:
- layer_out: bfloat16 [2048, 8, 2048], P(('sp', 'tp'), 'grp'), parts along dimension 1
There are 2 independent parts, one for each index of `grp`. A program takes and returns all parts, laid end to end along the dimension named above; an argument that names none is the same for every part. Nothing has to cross between parts.
All inputs are finite; a program needn't handle non-finite values.
Results may differ from a plain program's by a relative error of at most 0.013.
Values may be sent and summed in bfloat16 or wider, within the bound.
A program may use at most 128 MiB of HBM per device.

v0:
```python
import jax
import jax.numpy as jnp
from jax import lax
from jax.sharding import Mesh
from jax.sharding import PartitionSpec as P

KEY = 128
VAL = 128
BLOCK = 64
TP = ("tp_0", "tp_1")
SP_TP = ("sp", "tp_0", "tp_1")


norm_eps = 1e-06


def sent_together(arrays, axis, dim, along):
    widths = [a.shape[along] for a in arrays]
    both = jnp.concatenate(arrays, axis=along)
    out = lax.all_gather(both, axis, axis=dim, tiled=True)
    return tuple(jnp.split(out, [sum(widths[:k]) for k in range(1, len(widths))], axis=along))


def joined_along(parts, dim):
    lengths = list(parts.shape[1:])
    lengths[dim] *= parts.shape[0]
    return jnp.moveaxis(parts, 0, dim).reshape(lengths)


def from_everyone(x, axis):
    size = lax.axis_size(axis)
    return lax.all_to_all(jnp.broadcast_to(x[None], (size, *x.shape)), axis, 0, 0, tiled=True)


def collect(x, axis, dim):
    return joined_along(from_everyone(x, axis), dim)


def carried_in(x, axis, join, neutral, backward):
    count = lax.axis_size(axis)
    place = lax.axis_index(axis)
    ahead = count - 1 - place if backward else place
    gathered = jax.tree.map(
        lambda a, kind: lax.all_gather(a.astype(kind), axis), x, (jnp.bfloat16, jnp.bfloat16)
    )
    state = jax.tree.map(lambda a, e: jnp.zeros_like(a) + jnp.asarray(e, a.dtype), x, neutral)

    def one(turn, state):
        source = count - 1 - turn if backward else turn
        return join(
            state,
            jax.tree.map(
                lambda a, own: lax.dynamic_index_in_dim(a, source, 0, False).astype(own.dtype),
                gathered,
                x,
            ),
        )

    return lax.fori_loop(0, ahead, one, state)


def split_up(x, dim, size):
    lengths = x.shape
    parts = x.reshape(*lengths[:dim], size, lengths[dim] // size, *lengths[dim + 1 :])
    return jnp.moveaxis(parts, dim, 0)


def moved_by_axis(parts, axes, order):
    lengths = [lax.axis_size(a) for a in axes]
    parts = parts.reshape(*lengths, *parts.shape[1:])
    for k in order:
        parts = lax.all_to_all(parts, axes[k], split_axis=k, concat_axis=k, tiled=True)
    return parts.reshape(-1, *parts.shape[len(axes) :])


def stepwise_exchange(x, axes, order, split_dim, concat_dim):
    parts = split_up(x, split_dim, lax.axis_size(axes))
    return joined_along(moved_by_axis(parts, axes, order), concat_dim)


def split_blocks(array):
    return array.reshape(array.shape[0] // BLOCK, BLOCK, *array.shape[1:])


def prepare_chain(queries, key_cols, values, log_decay):
    query_blocks = split_blocks(queries)
    key_blocks = split_blocks(key_cols)
    value_blocks = split_blocks(values)
    running = jnp.cumsum(split_blocks(log_decay), axis=1)
    block_end = running[:, -1]
    block_state = jnp.einsum(
        "nsbhk,nsbhe->nbhke", key_blocks * jnp.exp(block_end[:, None] - running), value_blocks
    )
    carry_state = jnp.zeros_like(block_state[0])
    log_total = jnp.zeros_like(block_end[0])
    offsets = [log_total]
    carry_state = jnp.exp(block_end[0])[..., None] * carry_state + block_state[0]
    log_total = block_end[0]
    return (
        query_blocks,
        key_blocks,
        value_blocks,
        running,
        block_state,
        jnp.stack(offsets),
        log_total,
        carry_state,
    )


def local_pass(chain, carry_state):
    query_blocks, key_blocks, value_blocks, running, block_state = (
        chain[0],
        chain[1],
        chain[2],
        chain[3],
        chain[4],
    )
    block_len = running.shape[1]
    earlier_mask = jnp.arange(block_len)[:, None] >= jnp.arange(block_len)[None, :]
    here = running[0]
    anchor = here[:1]
    query_scaled = query_blocks[0] * jnp.exp(here - anchor)
    key_scaled = key_blocks[0] * jnp.exp(anchor - here)
    scores = jnp.einsum("tbhk,sbhk->bhts", query_scaled, key_scaled)
    scores = jnp.where(earlier_mask, scores, 0.0)
    within = jnp.einsum("bhts,sbhe->tbhe", scores, value_blocks[0])
    carried = jnp.einsum("tbhk,bhke->tbhe", query_blocks[0] * jnp.exp(here), carry_state)
    outputs = within + carried
    return outputs


def read_carried(chain, incoming):
    query_blocks, running, offsets = (chain[0], chain[3], chain[5])
    decayed = query_blocks * jnp.exp(running + offsets[:, None])
    result = jnp.einsum("ntbhk,bhke->ntbhe", decayed, incoming)
    return result.reshape(result.shape[0] * result.shape[1], *result.shape[2:])


def combine(earlier, later):
    return (earlier[0] + later[0], jnp.exp(later[0])[..., None] * earlier[1] + later[1])


def group_sums(flat_mixed, weight_lines, group_count):
    group_width = flat_mixed.shape[1] // group_count
    accumulated_total = jnp.zeros((flat_mixed.shape[0], weight_lines.shape[1]), jnp.float32)
    for tp_group in range(group_count):
        first_column = tp_group * group_width
        partial_value = jnp.dot(
            flat_mixed[:, first_column : first_column + group_width],
            weight_lines[first_column : first_column + group_width],
            preferred_element_type=jnp.float32,
        ).astype(jnp.bfloat16)
        accumulated_total = accumulated_total + lax.optimization_barrier(partial_value).astype(
            jnp.float32
        )
    return accumulated_total


def shards(
    tokens,
    norm_gain,
    w_query,
    w_value,
    w_fwd_gate,
    w_bwd_gate,
    w_out_gate,
    floor_gap,
    decay_shift,
    head_gain,
    w_out,
):
    token_f32 = tokens.astype(jnp.float32)
    scale_rows = lax.rsqrt(jnp.mean(token_f32 * token_f32, axis=-1, keepdims=True) + norm_eps)
    normed = (token_f32 * scale_rows * norm_gain).astype(jnp.bfloat16)
    weights = sent_together((w_query, w_value, w_fwd_gate, w_bwd_gate, w_out_gate), "sp", 0, 1)
    piece_rows = collect(normed, TP, 0)
    flat_rows = piece_rows.reshape(-1, piece_rows.shape[2])
    columns = [
        jnp.dot(flat_rows, matrix, preferred_element_type=jnp.float32).astype(jnp.bfloat16)
        for matrix in weights
    ]
    projected = lax.optimization_barrier(
        jnp.concatenate(columns, axis=1).reshape(piece_rows.shape[0], piece_rows.shape[1], -1)
    )
    key_width = w_query.shape[1]
    value_width = w_value.shape[1]
    heads_here = key_width // KEY
    extent_rows = projected.shape[0]
    seq_count = projected.shape[1]
    bounds_list = [
        0,
        key_width,
        key_width + value_width,
        2 * key_width + value_width,
        3 * key_width + value_width,
        3 * key_width + 2 * value_width,
    ]

    def section_part(position, feature_lanes):
        picked = projected[:, :, bounds_list[position] : bounds_list[position + 1]].astype(
            jnp.float32
        )
        return picked.reshape(extent_rows, seq_count, heads_here, feature_lanes)

    queries = jax.nn.silu(section_part(0, KEY))
    values = section_part(1, VAL)
    shift = decay_shift.reshape(extent_rows, seq_count, heads_here, KEY)
    key_fwd = floor_gap[0].reshape(heads_here, KEY) * jax.nn.sigmoid(-section_part(2, KEY))
    key_bwd = floor_gap[1].reshape(heads_here, KEY) * jax.nn.sigmoid(-section_part(3, KEY))
    decay_fwd = jnp.log1p(-key_fwd) + shift
    decay_bwd = jnp.log1p(-key_bwd) + shift
    fwd_chain = prepare_chain(queries, key_fwd, values, decay_fwd)
    bwd_chain = prepare_chain(queries[::-1], key_bwd[::-1], values[::-1], decay_bwd[::-1])
    identity_pair = (jnp.zeros_like(fwd_chain[6]), jnp.zeros_like(fwd_chain[7]))
    fwd_in = carried_in((fwd_chain[6], fwd_chain[7]), "sp", combine, identity_pair, False)[1]
    bwd_in = carried_in((bwd_chain[6], bwd_chain[7]), "sp", combine, identity_pair, True)[1]
    zero_state = jnp.zeros_like(fwd_in)
    out_fwd = local_pass(fwd_chain, zero_state) + read_carried(fwd_chain, fwd_in)
    out_bwd = local_pass(bwd_chain, zero_state) + read_carried(bwd_chain, bwd_in)
    combined = out_fwd + out_bwd[::-1]
    head_normed = (
        combined
        * lax.rsqrt(jnp.mean(combined * combined, axis=-1, keepdims=True) + norm_eps)
        * head_gain
    )
    gate_value = jax.nn.silu(projected[:, :, bounds_list[4] : bounds_list[5]].astype(jnp.float32))
    mixed = (head_normed.reshape(extent_rows, seq_count, value_width) * gate_value).astype(
        jnp.bfloat16
    )
    token_rows = stepwise_exchange(mixed, TP, (1, 0), 0, 2)
    flat_mixed = token_rows.reshape(-1, token_rows.shape[2])
    group_count = lax.axis_size(TP)
    weight_lines = lax.all_gather(w_out, TP, axis=0, tiled=True)
    accumulated_total = group_sums(
        flat_mixed, lax.all_gather(weight_lines, "sp", axis=1, tiled=True), group_count
    )
    result = accumulated_total.reshape(token_rows.shape[0], token_rows.shape[1], -1)
    return result.astype(jnp.bfloat16)


def solution(mesh):
    finer = Mesh(
        mesh.devices.reshape(mesh.shape["grp"], mesh.shape["sp"], 4, 2),
        ("grp", "sp", "tp_0", "tp_1"),
    )
    in_specs = (
        P(SP_TP, "grp", None),
        P(),
        P("sp", TP),
        P("sp", TP),
        P("sp", TP),
        P("sp", TP),
        P("sp", TP),
        P(None, TP),
        P("sp", "grp", TP),
        P(),
        P(TP, "sp"),
    )
    out_specs = P(SP_TP, "grp", None)
    return jax.shard_map(
        shards, mesh=finer, in_specs=in_specs, out_specs=out_specs, check_vma=False
    )
```

profile of v0, /device:TPU:36, one launch (start us, length us, event | category | flops | bytes accessed | tf_op | source)
XLA Modules:
  0.0 642.0 jit_solution(8801853182350276123)
XLA Ops:
  6.6 0.8 constant_dynamic-update-slice_fusion.4
  11.1 1.1 fusion.28
  12.1 1.0 fusion.30
  13.2 1.5 broadcast_in_dim.16
  14.7 43.8 %all-to-all-start = ((bf16[8,8,4,2048]{3,2,1,0:T(4,128)(2,1)}), bf16[8,8,4,2048]{3,2,1,0:T(4,128)(2,1)S(1)}, u32[]{:S(2)}, u32[]{:S(2)}) async-start(bf16[8,8,4,2048]{3,2,1,0:T(4,128)(2,1)} %broadcast_in_dim.16), calls=%async_computation | async-start | bytes 2097152 | tf_op jit(solution)/shard_map/all_to_all | solution.py:32
  58.5 1.1 reshape.238
  59.6 0.8 fusion.108
  60.4 10.8 %all-to-all-done = bf16[8,8,4,2048]{3,2,1,0:T(4,128)(2,1)S(1)} async-done(((bf16[8,8,4,2048]{3,2,1,0:T(4,128)(2,1)}), bf16[8,8,4,2048]{3,2,1,0:T(4,128)(2,1)S(1)}, u32[]{:S(2)}, u32[]{:S(2)}) %all-to-all-start) | async-done | bytes 1048608 | tf_op jit(solution)/shard_map/all_to_all | solution.py:32
  71.5 107.9 %all-gather.9.cloned.1.call-done = bf16[2048,1280]{1,0:T(8,128)(2,1)} async-done(((bf16[64,1280]{1,0:T(8,128)(2,1)}), bf16[2048,1280]{1,0:T(8,128)(2,1)}) %all-gather.9.cloned.1.call-update) | async-done | bytes 5242896 | tf_op jit(solution)/shard_map/all_gather | solution.py:20
  179.4 1.7 fusion.13
  181.1 1.7 fusion.12
  182.9 1.8 fusion.11
  184.7 1.8 fusion.10
  186.5 1.7 fusion.9
  189.9 1.1 fusion.1
  192.2 1.1 fusion
  193.5 12.9 %all_gather.30 = bf16[2048,64]{0,1:T(8,128)(2,1)} all-gather(bf16[256,64]{0,1:T(8,128)(2,1)S(1)} %copy-done.2), channel_id=1, replica_groups=mesh['grp'=2,'sp'=32,'tp_0'=4,'tp_1'=2] {'tp_0','tp_1'}, dimensions={0}, use_global_device_ids=true | all-gather | bytes 294912 | tf_op jit(solution)/shard_map/all_gather | solution.py:234
  206.9 53.4 %all-gather = bf16[32,1,4,2,128]{4,2,3,1,0:T(4,128)(2,1)S(1)} all-gather(bf16[1,1,4,2,128]{4,2,3,1,0:T(4,128)(2,1)S(1)} %copy.112), channel_id=2, replica_groups=mesh['grp'=2,'sp'=32,'tp_0'=4,'tp_1'=2] {'sp'}, dimensions={0}, use_global_device_ids=true | all-gather | bytes 67584 | tf_op jit(solution)/shard_map/all_gather | solution.py:44
  260.3 51.8 %all-gather.2 = bf16[32,1,4,2,128]{4,2,3,1,0:T(4,128)(2,1)S(1)} all-gather(bf16[1,1,4,2,128]{4,2,3,1,0:T(4,128)(2,1)S(1)} %copy.122), channel_id=4, replica_groups=mesh['grp'=2,'sp'=32,'tp_0'=4,'tp_1'=2] {'sp'}, dimensions={0}, use_global_device_ids=true | all-gather | bytes 67584 | tf_op jit(solution)/shard_map/all_gather | solution.py:44
  313.2 20.1 %all-gather.15.cloned.1.call-done = bf16[128,2,128,128]{3,2,1,0:T(8,128)(2,1)} async-done(((bf16[4,2,128,128]{3,2,1,0:T(8,128)(2,1)}), bf16[128,2,128,128]{3,2,1,0:T(8,128)(2,1)}) %all-gather.15.cloned.1.call-update) | async-done | bytes 8388624 | tf_op jit(solution)/shard_map/all_gather | solution.py:44
  333.4 40.2 %while.27 = (s32[]{:T(128)}, f32[4,2,128,128]{3,2,1,0:T(8,128)S(1)}, s32[]{:T(128)}, bf16[32,4,2,128]{3,1,2,0:T(4,128)(2,1)S(1)}, bf16[32,4,2,128,128]{4,3,2,1,0...) while((s32[]{:T(128)}, f32[4,2,128,128]{3,2,1,0:T(8,128)S(1)}, s32[]{:T(128)}, ...), condition=%wide.region_6.7_spmd, body=%wide.region_5.6_spmd.sunk | while | flops 394246 | bytes 1329299 | solution.py:59
  333.6 1.2 convert_add_fusion.5
  334.9 1.2 convert_add_fusion.5
  336.2 1.2 convert_add_fusion.5
  337.5 1.2 convert_add_fusion.5
  338.8 1.2 convert_add_fusion.5
  340.1 1.2 convert_add_fusion.5
  341.4 1.2 convert_add_fusion.5
  342.7 1.2 convert_add_fusion.5
  344.0 1.2 convert_add_fusion.5
  345.2 1.2 convert_add_fusion.5
  346.5 1.2 convert_add_fusion.5
  347.8 1.2 convert_add_fusion.5
  349.1 1.2 convert_add_fusion.5
  350.4 1.3 convert_add_fusion.5
  351.7 1.2 convert_add_fusion.5
  353.0 1.2 convert_add_fusion.5
  354.3 1.2 convert_add_fusion.5
  355.6 1.2 convert_add_fusion.5
  356.9 1.2 convert_add_fusion.5
  358.2 1.2 convert_add_fusion.5
  359.5 1.2 convert_add_fusion.5
  360.7 1.2 convert_add_fusion.5
  362.0 1.2 convert_add_fusion.5
  363.3 1.2 convert_add_fusion.5
  364.6 1.2 convert_add_fusion.5
  365.9 1.2 convert_add_fusion.5
  367.2 1.2 convert_add_fusion.5
  368.5 1.2 convert_add_fusion.5
  369.8 1.2 convert_add_fusion.5
  371.1 1.2 convert_add_fusion.5
  372.4 1.2 convert_add_fusion.5
  373.9 103.5 %all-gather.13.cloned.1.call-done = bf16[128,2,128,128]{3,2,1,0:T(8,128)(2,1)} async-done(((bf16[4,2,128,128]{3,2,1,0:T(8,128)(2,1)}), bf16[128,2,128,128]{3,2,1,0:T(8,128)(2,1)}) %all-gather.13.cloned.1.call-update) | async-done | bytes 8388624 | tf_op jit(solution)/shard_map/all_gather | solution.py:44
  478.7 3.9 all_to_all.15
  482.5 7.9 %all_to_all.16 = bf16[4,2,8,4,256]{4,2,3,1,0:T(8,128)(2,1)S(1)} all-to-all(bf16[4,2,8,4,256]{4,2,3,1,0:T(8,128)(2,1)S(1)} %copy.128), channel_id=1, replica_groups=mesh['grp'=2,'sp'=32,'tp_0'=4,'tp_1'=2] {'tp_0'}, dimensions={0} | all-to-all | bytes 262144 | tf_op jit(solution)/shard_map/all_to_all | solution.py:72
  490.5 130.9 %all-gather.11.cloned.1.call-done = bf16[2048,2048]{0,1:T(8,128)(2,1)} async-done(((bf16[2048,64]{0,1:T(8,128)(2,1)}), bf16[2048,2048]{0,1:T(8,128)(2,1)}) %all-gather.11.cloned.1.call-update) | async-done | bytes 8388624 | tf_op jit(solution)/shard_map/all_gather | solution.py:236
  621.5 1.6 convolution_convert_fusion.7
  623.1 1.6 convolution_convert_fusion.6
  624.7 1.6 convolution_convert_fusion.5
  626.4 1.6 convolution_convert_fusion.4
  628.0 1.6 convolution_convert_fusion.3
  629.7 1.6 convolution_convert_fusion.2
  631.3 1.6 convolution_convert_fusion.1
  632.9 1.6 convolution_convert_fusion
  (133 shorter events, 11.5 us)
Async XLA Ops:
  6.5 172.8 %all-gather.9.cloned.1.call-start = ((), (), s32[]{:S(2)}) async-start(), calls=%async_computation.3 | async-start | bytes 5406720 | tf_op jit(solution)/shard_map/all_gather | solution.py:20
  10.4 0.7 copy-start.1
  14.7 56.5 %all-to-all-start = ((bf16[8,8,4,2048]{3,2,1,0:T(4,128)(2,1)}), bf16[8,8,4,2048]{3,2,1,0:T(4,128)(2,1)S(1)}, u32[]{:S(2)}, u32[]{:S(2)}) async-start(bf16[8,8,4,2048]{3,2,1,0:T(4,128)(2,1)} %broadcast_in_dim.16), calls=%async_computation | async-start | bytes 2097152 | tf_op jit(solution)/shard_map/all_to_all | solution.py:32
  58.5 274.9 %all-gather.15.cloned.1.call-start = ((), (), s32[]{:S(2)}) async-start(), calls=%async_computation.6 | async-start | bytes 8650752 | tf_op jit(solution)/shard_map/all_gather | solution.py:44
  182.9 8.3 %copy-start = (f32[64,4,256]{2,1,0:T(4,128)S(1)}, f32[64,4,256]{2,1,0:T(4,128)}, u32[]{:S(2)}) copy-start(f32[64,4,256]{2,1,0:T(4,128)} %param.23) | copy-start | bytes 786436
  184.7 8.8 %copy-start.2 = (bf16[256,64]{0,1:T(8,128)(2,1)S(1)}, bf16[256,64]{0,1:T(8,128)(2,1)}, u32[]{:S(2)}) copy-start(bf16[256,64]{0,1:T(8,128)(2,1)} %param.25) | copy-start | bytes 98308
  191.1 286.3 %all-gather.13.cloned.1.call-start = ((), (), s32[]{:S(2)}) async-start(), calls=%async_computation.5 | async-start | bytes 8650752 | tf_op jit(solution)/shard_map/all_gather | solution.py:44
  193.4 428.1 %all-gather.11.cloned.1.call-start = ((), (), s32[]{:S(2)}) async-start(), calls=%async_computation.4 | async-start | bytes 8650752 | tf_op jit(solution)/shard_map/all_gather | solution.py:236
  333.4 144.4 %copy-start.3 = (f32[128]{0:T(128)S(1)}, f32[128]{0:T(128)}, u32[]{:S(2)}) copy-start(f32[128]{0:T(128)} %param.24) | copy-start | bytes 1540
Sparse Core Ops, SparseCore 0:
  11.2 168.1 all-gather.8
  191.2 142.1 all-gather.14
  335.4 141.9 all-gather.12
  479.4 142.0 all-gather.10
where the time goes:
time: 644 us; the launch traced here: 642 us
  waiting for transfers between devices  374 us (58%)
  blocking collectives  130 us (20%)
  starting transfers between devices  43.9 us (7%)
  other arithmetic  42.3 us (7%)
  matrix products  25.7 us (4%)
  between operations  13.6 us (2%)
  local copies, waits for them, and re-layouts  11.5 us (2%)
    all_gather x1, waiting for transfers between devices, shards(): lax.all_gather(weight_lines, 'sp', axis=1, tiled=True)  131 us
    all_gather x2, waiting for transfers between devices, carried_in(): lax.all_gather(a.astype(kind), axis)  124 us
    all_gather x1, waiting for transfers between devices, sent_together(): out = lax.all_gather(both, axis, axis=dim, tiled=True)  108 us
    all_gather x2, blocking collectives, carried_in(): lax.all_gather(a.astype(kind), axis)  105 us
    all_to_all x1, starting transfers between devices, from_everyone(): lax.all_to_all(jnp.broadcast_to(x[None], (size, *x.shape)), axis, 0, 0, t...  43.8 us
    add x31, other arithmetic, combine(): jnp.exp(later[0])[..., None] * earlier[1] + later[1]  38.1 us
    dot_general x8, matrix products, group_sums(): jnp.dot(flat_mixed[:, first_column:first_column + group_width], weight_li...  13.1 us
    all_gather x1, blocking collectives, shards(): weight_lines = lax.all_gather(w_out, TP, axis=0, tiled=True)  12.9 us
  transfers between devices with their start and end apart: 5, of which 5 were waited for; matrix products, arithmetic and copies ran while one was open for 8% of the time, Pallas kernels for 0%

commit v1 on v0

v1 whole, which is shorter than its diff:
```python
import functools

import jax
import jax.numpy as jnp
from jax import lax
from jax.experimental import pallas as pl
from jax.experimental.pallas import tpu as pltpu
from jax.sharding import PartitionSpec as P

MESH = pl.DeviceIdType.MESH
F32 = jnp.float32
BF16 = jnp.bfloat16
CH = 128
BLK = 4
SLOTS = 4
EPS = 1e-06


def dims(contract):
    return (contract, ((), ()))


def kernel(
    n_sp,
    n_tp,
    tokens,
    gain,
    w_query,
    w_value,
    w_fwd,
    w_bwd,
    w_gate,
    w_out,
    gap,
    shift,
    head_gain,
    out,
    weights,
    normed,
    qs,
    vs,
    kf,
    kb,
    rf,
    rb,
    gs,
    qe,
    inner,
    local,
    decay,
    before,
    decay_before,
    sent1,
    decay_sent,
    total,
    ahead,
    sent2,
    carried,
    mixed,
    mine,
    given,
    taken,
    summed,
    pieces,
    ring_send,
    ring_recv,
    y_send,
    y_recv,
    tok_send,
    tok_recv,
    d_send,
    d_recv,
    p1_send,
    p1_recv,
    p2_send,
    p2_recv,
    pair_send,
    pair_recv,
    x_send,
    x_recv,
):
    z = lax.axis_index("sp")
    tp = lax.axis_index("tp")
    grp = lax.axis_index("grp")
    parity = lax.rem(grp, 2)
    mate = grp + 1 - 2 * parity
    right, left = lax.rem(z + 1, n_sp), lax.rem(z + n_sp - 1, n_sp)
    n_x = n_tp // 2
    core, x = lax.rem(tp, 2), tp // 2
    wrows, width = w_query.shape
    step_pos, seqs, model = tokens.shape
    span = shift.shape[0]
    heads = width // CH
    chunks = seqs * heads
    n_blocks = n_sp // BLK
    block_rows = step_pos * seqs
    half = n_sp // 2

    def spot(t):
        return (t % 2) * n_x + t // 2

    here = spot(tp)

    own_rows = pl.ds(pl.multiple_of(z * wrows, wrows), wrows)
    for m, ref in enumerate((w_value, w_fwd, w_bwd, w_gate, w_query)):
        weights[m, own_rows, :] = ref[...]
    eye = (
        lax.broadcasted_iota(jnp.int32, (width, width), 0)
        == lax.broadcasted_iota(jnp.int32, (width, width), 1)
    ).astype(F32).astype(BF16)
    weights[5, own_rows, :] = lax.dot_general(
        w_out[...], eye, dims(((0,), (0,))), preferred_element_type=F32
    ).astype(BF16)

    barrier = pltpu.get_barrier_semaphore()
    greeted = 0
    for peer in (
        [{"sp": right}, {"sp": left}]
        + [{"sp": lax.rem(z + BLK, n_sp)}, {"sp": lax.rem(z + n_sp - BLK, n_sp)}]
        + [{"tp": lax.rem(tp + d, n_tp)} for d in range(1, n_tp)]
        + [{"grp": mate}]
    ):
        pl.semaphore_signal(barrier, inc=1, device_id=peer, device_id_type=MESH)
        greeted += 1
    pl.semaphore_wait(barrier, greeted)

    def matrix(slot, par):
        return slot if slot < 2 else slot + 2 * par

    def block(slot, origin, par):
        return weights.at[
            matrix(slot, par), pl.ds(pl.multiple_of(origin * wrows, wrows), wrows)
        ]

    def hop(slot, origin, step, way):
        ref = block(slot, origin, parity)
        return pltpu.make_async_remote_copy(
            src_ref=ref,
            dst_ref=ref,
            send_sem=ring_send.at[way, slot],
            recv_sem=ring_recv.at[way, slot, step],
            device_id={"sp": left if way else right},
            device_id_type=MESH,
        )

    def over(ref, k):
        return pltpu.make_async_remote_copy(
            src_ref=ref,
            dst_ref=ref,
            send_sem=y_send.at[k],
            recv_sem=y_recv.at[k],
            device_id={"grp": mate},
            device_id_type=MESH,
        )

    for slot in range(SLOTS):
        for way in (0, 1):
            hop(slot, z, 1, way).start()

    tok = tokens[...].astype(F32)
    rows = []
    for b in range(seqs):
        part = tok[:, b, :]
        scale = lax.rsqrt(jnp.mean(part * part, axis=-1, keepdims=True) + EPS)
        rows.append(part * scale * gain[...])
    tok_block = pl.ds(pl.multiple_of(here * block_rows, block_rows), block_rows)
    normed[tok_block, :] = jnp.concatenate(rows, axis=0).astype(BF16)

    def token_copy(ref, peer):
        return pltpu.make_async_remote_copy(
            src_ref=ref,
            dst_ref=ref,
            send_sem=tok_send,
            recv_sem=tok_recv,
            device_id={"tp": peer},
            device_id_type=MESH,
        )

    for d in range(1, n_tp):
        token_copy(normed.at[tok_block], lax.rem(tp + d, n_tp)).start()

    def arrive(slot, step, way, forward):
        origin = lax.rem(z + step, n_sp) if way else lax.rem(z + n_sp - step, n_sp)
        hop(slot, origin, step, way).wait_recv()
        if forward is True:
            hop(slot, origin, step + 1, way).start()
        elif forward is not False:
            @pl.when(forward)
            def _():
                hop(slot, origin, step + 1, way).start()
        if slot >= 2:
            over(block(slot, origin, parity), slot - 2).start()

    def ring_step(step, carry):
        for slot in range(SLOTS):
            arrive(slot, step, 0, True)
            arrive(slot, step, 1, step < half - 1)
        return carry

    lax.fori_loop(1, half, ring_step, 0)
    for slot in range(SLOTS):
        arrive(slot, half, 0, False)

    others = block_rows * (n_tp - 1)
    token_copy(normed.at[pl.ds(0, others)], tp).wait_recv()

    def project(m):
        return (
            jnp.dot(normed[...], weights[m], preferred_element_type=F32)
            .astype(BF16)
            .astype(F32)
        )

    def by_sequence(ref, value):
        for t in range(n_tp):
            for b in range(seqs):
                first = spot(t) * block_rows + b * step_pos
                ref[b, t * step_pos : (t + 1) * step_pos, :] = value[
                    first : first + step_pos, :
                ]

    def silu(u):
        return u / (1.0 + jnp.exp(-u))

    by_sequence(vs, project(0))
    by_sequence(kf, gap[0:1, :] / (1.0 + jnp.exp(project(1))))
    for k in range(2):
        theirs = weights.at[2 + k + 2 * (1 - parity), pl.ds(0, wrows * (n_sp - 1))]
        over(theirs, k).wait_recv()
    by_sequence(kb, gap[1:2, :] / (1.0 + jnp.exp(project(2))))

    at_row = lax.broadcasted_iota(jnp.int32, (span, span), 0)
    at_col = lax.broadcasted_iota(jnp.int32, (span, span), 1)
    lower = (at_row >= at_col).astype(F32)
    upper = (at_row <= at_col).astype(F32)
    for b in range(seqs):
        moved = shift[:, b, :]
        fwd_key, bwd_key = kf[b], kb[b]
        fwd_run = jnp.dot(
            lower,
            jnp.log1p(-fwd_key) + moved,
            precision=lax.Precision.HIGHEST,
            preferred_element_type=F32,
        )
        bwd_run = jnp.dot(
            upper,
            jnp.log1p(-bwd_key) + moved,
            precision=lax.Precision.HIGHEST,
            preferred_element_type=F32,
        )
        rf[b] = fwd_run
        rb[b] = bwd_run
        fwd_end, bwd_end = fwd_run[span - 1 : span, :], bwd_run[0:1, :]
        keys = jnp.concatenate(
            [fwd_key * jnp.exp(fwd_end - fwd_run), bwd_key * jnp.exp(bwd_end - bwd_run)],
            axis=1,
        ).astype(BF16)
        states = lax.dot_general(
            vs[b].astype(BF16), keys, dims(((0,), (0,))), preferred_element_type=F32
        )
        for h in range(heads):
            c = b * heads + h
            lanes = slice(h * CH, (h + 1) * CH)
            for d, end in enumerate((fwd_end, bwd_end)):
                local[d, c] = states[lanes, d * width + h * CH : d * width + (h + 1) * CH]
                decay[d, c : c + 1, :] = jnp.exp(end[:, lanes])

    def ends(d):
        place = (n_sp - 1 - z) if d == 1 else z
        return place // BLK, lax.rem(place, BLK), (-1 if d == 1 else 1)

    def scan_copy(src, dst, send, recv, target):
        return pltpu.make_async_remote_copy(
            src_ref=src,
            dst_ref=dst,
            send_sem=send,
            recv_sem=recv,
            device_id={"sp": target},
            device_id_type=MESH,
        )

    def near(d, way, c=None):
        if c is None:
            return scan_copy(
                decay_sent.at[d], decay_before.at[d], d_send.at[d], d_recv.at[d], z + way
            )
        return scan_copy(
            sent1.at[d, c], before.at[d, c], p1_send.at[d], p1_recv.at[d, c], z + way
        )

    def far(d, way, c):
        return scan_copy(
            sent2.at[d, c], ahead.at[d, c], p2_send.at[d, 0], p2_recv.at[d, c], z + BLK * way
        )

    def down(d, way, c):
        return scan_copy(
            sent2.at[d, c], ahead.at[d, c], p2_send.at[d, 1], p2_recv.at[d, c], z + way
        )

    def relay(d, way, c):
        return scan_copy(
            ahead.at[d, c], ahead.at[d, c], p2_send.at[d, 1], p2_recv.at[d, c], z + way
        )

    for d in (0, 1):
        jj, rr, way = ends(d)

        @pl.when(jj == 0)
        def _():
            ahead[d] = jnp.zeros(ahead.shape[1:], ahead.dtype)

        @pl.when(rr == 0)
        def _():
            before[d] = jnp.zeros(before.shape[1:], before.dtype)
            decay_before[d] = jnp.ones(decay_before.shape[1:], F32)

        @pl.when(rr > 0)
        def _():
            near(d, way).wait_recv()

        decay_sent[d] = decay_before[d] * decay[d]

        @pl.when(rr < BLK - 1)
        def _():
            near(d, way).start()

    def first_pass(c, carry):
        for d in (0, 1):
            jj, rr, way = ends(d)

            @pl.when(rr > 0)
            def _():
                near(d, way, c).wait_recv()

            joined = decay[d, pl.ds(c, 1), :] * before[d, c].astype(F32) + local[d, c]

            @pl.when(rr < BLK - 1)
            def _():
                sent1[d, c] = joined.astype(BF16)
                near(d, way, c).start()

            @pl.when(rr == BLK - 1)
            def _():
                total[d, c] = joined

                @pl.when(jj == 0)
                def _():
                    sent2[d, c] = joined.astype(BF16)
                    far(d, way, c).start()
                    down(d, way, c).start()

        return carry

    lax.fori_loop(0, chunks, first_pass, 0)

    def second_pass(d):
        jj, rr, way = ends(d)

        def each(c, carry):
            @pl.when(jj > 0)
            def _():
                far(d, way, c).wait_recv()

            @pl.when((rr == BLK - 1) & (jj > 0) & (jj < n_blocks - 1))
            def _():
                joined = (
                    decay_sent[d, pl.ds(c, 1), :] * ahead[d, c].astype(F32) + total[d, c]
                )
                sent2[d, c] = joined.astype(BF16)
                far(d, way, c).start()
                down(d, way, c).start()

            @pl.when((rr < BLK - 2) & (jj > 0))
            def _():
                relay(d, way, c).start()

            carried[c, :, d * CH : (d + 1) * CH] = (
                decay_before[d, pl.ds(c, 1), :] * ahead[d, c].astype(F32)
                + before[d, c].astype(F32)
            ).astype(BF16)
            return carry

        lax.fori_loop(0, chunks, each, 0)

    def inside():
        by_sequence(qs, silu(project(4)))
        by_sequence(gs, silu(project(3)))
        middle = span // 2 - 1
        for b in range(seqs):
            query, fwd_run, bwd_run = qs[b], rf[b], rb[b]
            fwd_mid, bwd_mid = fwd_run[middle : middle + 1, :], bwd_run[middle : middle + 1, :]
            fwd_q = (query * jnp.exp(fwd_run - fwd_mid)).astype(BF16)
            bwd_q = (query * jnp.exp(bwd_run - bwd_mid)).astype(BF16)
            fwd_k = (kf[b] * jnp.exp(fwd_mid - fwd_run)).astype(BF16)
            bwd_k = (kb[b] * jnp.exp(bwd_mid - bwd_run)).astype(BF16)
            fwd_e = (query * jnp.exp(fwd_run)).astype(BF16)
            bwd_e = (query * jnp.exp(bwd_run)).astype(BF16)
            value = vs[b].astype(BF16)
            for h in range(heads):
                c = b * heads + h
                lanes = slice(h * CH, (h + 1) * CH)
                fwd_s = lax.dot_general(
                    fwd_q[:, lanes], fwd_k[:, lanes], dims(((1,), (1,))), preferred_element_type=F32
                )
                bwd_s = lax.dot_general(
                    bwd_q[:, lanes], bwd_k[:, lanes], dims(((1,), (1,))), preferred_element_type=F32
                )
                scores = jnp.where(at_row >= at_col, fwd_s, 0.0) + jnp.where(
                    at_row <= at_col, bwd_s, 0.0
                )
                inner[c] = jnp.dot(
                    scores.astype(BF16), value[:, lanes], preferred_element_type=F32
                )
                qe[c] = jnp.concatenate([fwd_e[:, lanes], bwd_e[:, lanes]], axis=1)

    low = z < half

    @pl.when(low)
    def _():
        second_pass(0)

    @pl.when(jnp.logical_not(low))
    def _():
        second_pass(1)

    inside()

    @pl.when(low)
    def _():
        second_pass(1)

    @pl.when(jnp.logical_not(low))
    def _():
        second_pass(0)

    for b in range(seqs):
        for h in range(heads):
            c = b * heads + h
            both = inner[c] + lax.dot_general(
                qe[c], carried[c], dims(((1,), (1,))), preferred_element_type=F32
            )
            scale = lax.rsqrt(jnp.mean(both * both, axis=-1, keepdims=True) + EPS)
            gated = both * scale * head_gain[...] * gs[b, :, h * CH : (h + 1) * CH]
            for t in range(n_tp):
                first = spot(t) * block_rows + b * step_pos
                mixed[first : first + step_pos, h * CH : (h + 1) * CH] = gated[
                    t * step_pos : (t + 1) * step_pos, :
                ]

    side = n_x * block_rows

    def partial(which):
        lines = pl.ds(pl.multiple_of(which * side, side), side)
        return lax.dot_general(
            mixed[lines, :].astype(BF16),
            weights[5],
            dims(((1,), (1,))),
            preferred_element_type=F32,
        )

    given[...] = partial(1 - core).astype(BF16)
    pair = pltpu.make_async_remote_copy(
        src_ref=given,
        dst_ref=taken,
        send_sem=pair_send,
        recv_sem=pair_recv,
        device_id={"tp": tp + 1 - 2 * core},
        device_id_type=MESH,
    )
    pair.start()
    mine[...] = partial(core)
    pair.wait_recv()

    def piece(dest, d):
        lines = pl.ds(pl.multiple_of(dest * block_rows, block_rows), block_rows)
        return pltpu.make_async_remote_copy(
            src_ref=summed.at[lines],
            dst_ref=pieces.at[d - 1],
            send_sem=x_send.at[d - 1],
            recv_sem=x_recv.at[d - 1],
            device_id={"tp": dest * 2 + core},
            device_id_type=MESH,
        )

    order = [2, 1, 3] if n_x == 4 else list(range(1, n_x))
    for d in order:
        dest = lax.rem(x + d, n_x)
        lines = pl.ds(pl.multiple_of(dest * block_rows, block_rows), block_rows)
        summed[lines, :] = (mine[lines, :] + taken[lines, :].astype(F32)).astype(BF16)
        piece(dest, d).start()
    own_lines = pl.ds(pl.multiple_of(x * block_rows, block_rows), block_rows)
    result = mine[own_lines, :] + taken[own_lines, :].astype(F32)
    for d in range(1, n_x):
        piece(x, d).wait_recv()
        result = result + pieces[d - 1].astype(F32)
    out[...] = result.astype(BF16)

    for slot in range(SLOTS):
        for way in (0, 1):
            length = wrows * (half - way)
            ref = weights.at[matrix(slot, parity), pl.ds(0, length)]
            pltpu.make_async_remote_copy(
                src_ref=ref,
                dst_ref=ref,
                send_sem=ring_send.at[way, slot],
                recv_sem=ring_recv.at[way, slot, 0],
                device_id={"sp": right},
                device_id_type=MESH,
            ).wait_send()
    for k in range(2):
        over(weights.at[k, pl.ds(0, wrows * (n_sp - 1))], k).wait_send()
    token_copy(normed.at[pl.ds(0, others)], tp).wait_send()
    for d in (0, 1):
        jj, rr, way = ends(d)

        @pl.when(rr < BLK - 1)
        def _():
            near(d, way).wait_send()
            scan_copy(sent1.at[d], before.at[d], p1_send.at[d], p1_recv.at[d, 0], z).wait_send()

        leads = (rr == BLK - 1) & (jj < n_blocks - 1)

        @pl.when(leads)
        def _():
            scan_copy(sent2.at[d], ahead.at[d], p2_send.at[d, 0], p2_recv.at[d, 0], z).wait_send()

        @pl.when(leads | ((rr < BLK - 2) & (jj > 0)))
        def _():
            scan_copy(sent2.at[d], ahead.at[d], p2_send.at[d, 1], p2_recv.at[d, 0], z).wait_send()

    pair.wait_send()
    for d in range(1, n_x):
        piece(lax.rem(x + d, n_x), d).wait_send()


def shards(
    n_sp,
    n_tp,
    tokens,
    norm_gain,
    w_query,
    w_value,
    w_fwd_gate,
    w_bwd_gate,
    w_out_gate,
    floor_gap,
    decay_shift,
    head_gain,
    w_out,
):
    step_pos, seqs, model = tokens.shape
    wrows, width = w_query.shape
    span = decay_shift.shape[0]
    chunks = seqs * (width // CH)
    rows = step_pos * seqs
    all_rows = rows * n_tp
    n_x = n_tp // 2
    f32_rows = pltpu.VMEM((seqs, span, width), F32)
    vmem = pl.BlockSpec(memory_space=pltpu.VMEM)
    dma = pltpu.SemaphoreType.DMA
    result = pl.pallas_call(
        functools.partial(kernel, n_sp, n_tp),
        out_shape=jax.ShapeDtypeStruct((rows, model), BF16),
        in_specs=[vmem] * 11,
        out_specs=vmem,
        scratch_shapes=[
            pltpu.VMEM((6, wrows * n_sp, width), BF16),
            pltpu.VMEM((all_rows, model), BF16),
            f32_rows,
            f32_rows,
            f32_rows,
            f32_rows,
            f32_rows,
            f32_rows,
            f32_rows,
            pltpu.VMEM((chunks, span, 2 * CH), BF16),
            pltpu.VMEM((chunks, span, CH), F32),
            pltpu.VMEM((2, chunks, CH, CH), F32),
            pltpu.VMEM((2, chunks, CH), F32),
            pltpu.VMEM((2, chunks, CH, CH), BF16),
            pltpu.VMEM((2, chunks, CH), F32),
            pltpu.VMEM((2, chunks, CH, CH), BF16),
            pltpu.VMEM((2, chunks, CH), F32),
            pltpu.VMEM((2, chunks, CH, CH), F32),
            pltpu.VMEM((2, chunks, CH, CH), BF16),
            pltpu.VMEM((2, chunks, CH, CH), BF16),
            pltpu.VMEM((chunks, CH, 2 * CH), BF16),
            pltpu.VMEM((all_rows, width), F32),
            pltpu.VMEM((n_x * rows, model), F32),
            pltpu.VMEM((n_x * rows, model), BF16),
            pltpu.VMEM((n_x * rows, model), BF16),
            pltpu.VMEM((n_x * rows, model), BF16),
            pltpu.VMEM((n_x - 1, rows, model), BF16),
            dma((2, SLOTS)),
            dma((2, SLOTS, n_sp // 2 + 1)),
            dma((2,)),
            dma((2,)),
            dma,
            dma,
            dma((2,)),
            dma((2,)),
            dma((2,)),
            dma((2, chunks)),
            dma((2, 2)),
            dma((2, chunks)),
            dma,
            dma,
            dma((n_x - 1,)),
            dma((n_x - 1,)),
        ],
        compiler_params=pltpu.CompilerParams(
            collective_id=0, has_side_effects=True, vmem_limit_bytes=60 * 1024 * 1024
        ),
        name="mixer",
    )(
        tokens,
        norm_gain.reshape(1, -1),
        w_query,
        w_value,
        w_fwd_gate,
        w_bwd_gate,
        w_out_gate,
        w_out,
        floor_gap,
        decay_shift,
        head_gain.reshape(1, -1),
    )
    return result.reshape(seqs, step_pos, model).transpose(1, 0, 2)


def solution(mesh):
    in_specs = (
        P(("sp", "tp"), "grp", None),
        P(),
        P("sp", "tp"),
        P("sp", "tp"),
        P("sp", "tp"),
        P("sp", "tp"),
        P("sp", "tp"),
        P(None, "tp"),
        P("sp", "grp", "tp"),
        P(),
        P("tp", "sp"),
    )
    return jax.shard_map(
        functools.partial(shards, mesh.shape["sp"], mesh.shape["tp"]),
        mesh=mesh,
        in_specs=in_specs,
        out_specs=P(("sp", "tp"), "grp", None),
        check_vma=False,
    )
```

time: 644 us -> 321 us (0.50)
  the two profiles are of different devices: /device:TPU:36 before, /device:TPU:97 now
where the time goes in v1:
time: 321 us; the launch traced here: 320 us
  Pallas kernels  317 us (99%)
    pallas_call x1, Pallas kernels, shards(): pl.pallas_call(functools.partial(kernel, n_sp, n_tp), out_shape=jax.Shape...  317 us

profile of v1, /device:TPU:97, one launch (start us, length us, event | category | flops | bytes accessed | tf_op | source)
XLA Modules:
  0.0 320.5 jit_solution(9132111941190587352)
XLA Ops:
  0.0 1.5 copy.12.w_out
  1.5 317.3 %mixer.1 = bf16[32,2048]{1,0:T(8,128)(2,1)} custom-call(bf16[8,4,2048]{2,1,0:T(4,128)(2,1)} %tokens.1, f32[1,2048]{1,0:T(1,128)} %bitcast.7, bf16[64,256]{1,0:T(8,128)(2,1)} %w_query.1, bf16[64,256]{1,0:T(8,128)(2,1)} %w_value.1, bf16[64,256]{1,0:T(8,128)(2,1)} %w_fwd.1, bf16[64,256]{1,0:T(8,128)(2,1)} %w_bwd.1, bf16[64,256]{1,0:T(8,128)(2,1)} %w_gate.1, ...), custom_call_target="tpu_custom_call" | custom-call | tf_op jit(solution)/shard_map/mixer/pallas_call | solution.py:562
  318.8 1.7 copy.15

commit v2 on v1

--- a/solution.py
+++ b/solution.py
@@ -49,6 +49,7 @@
     local,
     decay,
     before,
+    decay_in,
     decay_before,
     sent1,
     decay_sent,
@@ -279,11 +280,12 @@
             device_id_type=MESH,
         )
 
-    def near(d, way, c=None):
-        if c is None:
-            return scan_copy(
-                decay_sent.at[d], decay_before.at[d], d_send.at[d], d_recv.at[d], z + way
-            )
+    def factor(d, way, j):
+        return scan_copy(
+            decay.at[d], decay_in.at[d, j - 1], d_send.at[d, j - 1], d_recv.at[d, j - 1], z + j * way
+        )
+
+    def near(d, way, c):
         return scan_copy(
             sent1.at[d, c], before.at[d, c], p1_send.at[d], p1_recv.at[d, c], z + way
         )
@@ -313,21 +315,17 @@
         @pl.when(rr == 0)
         def _():
             before[d] = jnp.zeros(before.shape[1:], before.dtype)
-            decay_before[d] = jnp.ones(decay_before.shape[1:], F32)
-
-        @pl.when(rr > 0)
-        def _():
-            near(d, way).wait_recv()
-
-        decay_sent[d] = decay_before[d] * decay[d]
-
-        @pl.when(rr < BLK - 1)
-        def _():
-            near(d, way).start()
-
-    def first_pass(c, carry):
-        for d in (0, 1):
-            jj, rr, way = ends(d)
+
+        for j in range(1, BLK):
+
+            @pl.when(rr + j < BLK)
+            def _():
+                factor(d, way, j).start()
+
+    def first_pass(d):
+        jj, rr, way = ends(d)
+
+        def each(c, carry):
 
             @pl.when(rr > 0)
             def _():
@@ -350,9 +348,33 @@
                     far(d, way, c).start()
                     down(d, way, c).start()
 
-        return carry
-
-    lax.fori_loop(0, chunks, first_pass, 0)
+            return carry
+
+        lax.fori_loop(0, chunks, each, 0)
+
+    early = lax.rem(z, BLK) < BLK // 2
+
+    @pl.when(early)
+    def _():
+        first_pass(0)
+        first_pass(1)
+
+    @pl.when(jnp.logical_not(early))
+    def _():
+        first_pass(1)
+        first_pass(0)
+
+    for d in (0, 1):
+        jj, rr, way = ends(d)
+        decay_before[d] = jnp.ones(decay_before.shape[1:], F32)
+        for j in range(1, BLK):
+
+            @pl.when(rr >= j)
+            def _():
+                factor(d, way, j).wait_recv()
+                decay_before[d] = decay_before[d] * decay_in[d, j - 1]
+
+        decay_sent[d] = decay_before[d] * decay[d]
 
     def second_pass(d):
         jj, rr, way = ends(d)
@@ -516,8 +538,13 @@
 
         @pl.when(rr < BLK - 1)
         def _():
-            near(d, way).wait_send()
             scan_copy(sent1.at[d], before.at[d], p1_send.at[d], p1_recv.at[d, 0], z).wait_send()
+
+        for j in range(1, BLK):
+
+            @pl.when(rr + j < BLK)
+            def _():
+                factor(d, way, j).wait_send()
 
         leads = (rr == BLK - 1) & (jj < n_blocks - 1)
 
@@ -579,6 +606,7 @@
             pltpu.VMEM((2, chunks, CH, CH), F32),
             pltpu.VMEM((2, chunks, CH), F32),
             pltpu.VMEM((2, chunks, CH, CH), BF16),
+            pltpu.VMEM((2, BLK - 1, chunks, CH), F32),
             pltpu.VMEM((2, chunks, CH), F32),
             pltpu.VMEM((2, chunks, CH, CH), BF16),
             pltpu.VMEM((2, chunks, CH), F32),
@@ -598,8 +626,8 @@
             dma((2,)),
             dma,
             dma,
-            dma((2,)),
-            dma((2,)),
+            dma((2, BLK - 1)),
+            dma((2, BLK - 1)),
             dma((2,)),
             dma((2, chunks)),
             dma((2, 2)),

time: 321 us -> 181 us (0.56)
  Pallas kernels: 317 us -> 177 us
    pallas_call x1, Pallas kernels: 317 us -> 177 us  [shards(): pl.pallas_call(functools.partial(kernel, n_sp, n_tp), out_shape=jax.Shape...]
where the time goes in v2:
time: 181 us; the launch traced here: 180 us
  Pallas kernels  177 us (98%)
  local copies, waits for them, and re-layouts  3.15 us (2%)
    pallas_call x1, Pallas kernels, shards(): pl.pallas_call(functools.partial(kernel, n_sp, n_tp), out_shape=jax.Shape...  177 us

profile of v2, /device:TPU:97, one launch (start us, length us, event | category | flops | bytes accessed | tf_op | source)
XLA Modules:
  0.0 180.5 jit_solution(3361020177815528026)
XLA Ops:
  0.0 1.5 copy.12.w_out
  1.5 177.3 %mixer.1 = bf16[32,2048]{1,0:T(8,128)(2,1)} custom-call(bf16[8,4,2048]{2,1,0:T(4,128)(2,1)} %tokens.1, f32[1,2048]{1,0:T(1,128)} %bitcast.7, bf16[64,256]{1,0:T(8,128)(2,1)} %w_query.1, bf16[64,256]{1,0:T(8,128)(2,1)} %w_value.1, bf16[64,256]{1,0:T(8,128)(2,1)} %w_fwd.1, bf16[64,256]{1,0:T(8,128)(2,1)} %w_bwd.1, bf16[64,256]{1,0:T(8,128)(2,1)} %w_gate.1, ...), custom_call_target="tpu_custom_call" | custom-call | tf_op jit(solution)/shard_map/mixer/pallas_call | solution.py:589
  178.8 1.7 copy.15

commit v3 on v1

v3 whole, which is shorter than its diff:
```python
import functools

import jax
import jax.numpy as jnp
from jax import lax
from jax.experimental import pallas as pl
from jax.experimental.pallas import tpu as pltpu
from jax.sharding import PartitionSpec as P

MESH = pl.DeviceIdType.MESH
F32 = jnp.float32
BF16 = jnp.bfloat16
CH = 128
BLK = 4
RING = 3
CARRIER = 1
PARTS = 2
STRIPS = 2
LAG = 7
EPS = 1e-06


def dims(contract):
    return (contract, ((), ()))


def kernel(
    n_sp,
    n_tp,
    tokens,
    gain,
    w_query,
    w_value,
    w_fwd,
    w_bwd,
    w_gate,
    w_out,
    gap,
    shift,
    head_gain,
    out,
    weights,
    others,
    normed,
    gap_there,
    shift_there,
    vs_there,
    kf_there,
    kb_there,
    rf_there,
    rb_there,
    qs,
    vs,
    kf,
    kb,
    rf,
    rb,
    gs,
    qe,
    inner,
    local,
    decay,
    before,
    decay_in,
    decay_before,
    sent1,
    decay_sent,
    total,
    ahead,
    sent2,
    carried,
    mixed,
    mine,
    given,
    taken,
    summed,
    pieces,
    ring_send,
    ring_recv,
    first_send,
    push_send,
    push_recv,
    y_send,
    y_recv,
    tok_send,
    tok_recv,
    lend_send,
    lend_recv,
    own_send,
    own_recv,
    hand_send,
    hand_recv,
    back_send,
    back_recv,
    d_send,
    d_recv,
    p1_send,
    p1_recv,
    p2_send,
    p2_recv,
    pair_send,
    pair_recv,
    x_send,
    x_recv,
):
    z = lax.axis_index("sp")
    tp = lax.axis_index("tp")
    grp = lax.axis_index("grp")
    parity = lax.rem(grp, 2)
    mate = grp + 1 - 2 * parity
    right, left = lax.rem(z + 1, n_sp), lax.rem(z + n_sp - 1, n_sp)
    n_x = n_tp // 2
    core, x = lax.rem(tp, 2), tp // 2
    partner = tp + 1 - 2 * core
    carrier = core == CARRIER
    wrows, width = w_query.shape
    step_pos, seqs, model = tokens.shape
    span = shift.shape[0]
    heads = width // CH
    chunks = seqs * heads
    n_blocks = n_sp // BLK
    block_rows = step_pos * seqs
    half = n_sp // 2

    def spot(t):
        return (t % 2) * n_x + t // 2

    here = spot(tp)

    own_rows = pl.ds(pl.multiple_of(z * wrows, wrows), wrows)
    for m, ref in enumerate((w_value, w_fwd, w_bwd, w_out, w_gate, w_query)):
        weights[m, own_rows, :] = ref[...]

    barrier = pltpu.get_barrier_semaphore()
    greeted = 0
    for peer in (
        [{"sp": a, "tp": b} for a in (right, left) for b in (tp, partner)]
        + [{"tp": lax.rem(tp + d, n_tp)} for d in range(1, n_tp)]
        + [{"grp": mate, "tp": b} for b in (tp, partner)]
    ):
        pl.semaphore_signal(barrier, inc=1, device_id=peer, device_id_type=MESH)
        greeted += 1
    pl.semaphore_wait(barrier, greeted)

    share = wrows // PARTS

    def block(ref, m, origin, p):
        return ref.at[m, pl.ds(pl.multiple_of(origin * wrows + p * share, share), share)]

    def which(i):
        return i * (1 + parity)

    def held(base, i, owner, origin, p):
        if owner:
            return block(others, which(i), origin, p)
        return block(weights, base + which(i), origin, p)

    def hop(base, i, owner, origin, step, way, p):
        ref = held(base, i, owner, origin, p)
        return pltpu.make_async_remote_copy(
            src_ref=ref,
            dst_ref=ref,
            send_sem=ring_send.at[way, i, owner],
            recv_sem=ring_recv.at[way, i, owner, step, p],
            device_id={"sp": left if way else right},
            device_id_type=MESH,
        )

    def enter(base, i, way, p):
        return pltpu.make_async_remote_copy(
            src_ref=block(weights, base + which(i), z, p),
            dst_ref=block(others, which(i), z, p),
            send_sem=first_send.at[way, i, p],
            recv_sem=ring_recv.at[way, i, 1, 1, p],
            device_id={"sp": left if way else right, "tp": partner},
            device_id_type=MESH,
        )

    def push(src, dst, i):
        return pltpu.make_async_remote_copy(
            src_ref=src,
            dst_ref=dst,
            send_sem=push_send.at[i],
            recv_sem=push_recv.at[i],
            device_id={"tp": partner},
            device_id_type=MESH,
        )

    def over(src, dst, base, owner):
        return pltpu.make_async_remote_copy(
            src_ref=src,
            dst_ref=dst,
            send_sem=y_send.at[owner],
            recv_sem=y_recv.at[2 if base else owner],
            device_id={"grp": mate, "tp": partner if base and owner else tp},
            device_id_type=MESH,
        )

    def open_ring(base):
        for i in range(2):
            for p in range(PARTS):
                for way in (0, 1):
                    hop(base, i, 0, z, 1, way, p).start()

    def join_ring(base):
        for i in range(2):
            for p in range(PARTS):
                for way in (0, 1):
                    enter(base, i, way, p).start()

    def arrive(base, i, owner, step, way, p, forward):
        origin = lax.rem(z + step, n_sp) if way else lax.rem(z + n_sp - step, n_sp)
        hop(base, i, owner, origin, step, way, p).wait_recv()
        if forward is True:
            hop(base, i, owner, origin, step + 1, way, p).start()
        elif forward is not False:

            @pl.when(forward)
            def _():
                hop(base, i, owner, origin, step + 1, way, p).start()

        mine = held(base, i, owner, origin, p)
        home = block(weights, base + which(i), origin, p)
        if i:
            over(mine, home if base else mine, base, owner).start()
        if base and owner:
            push(mine, home, i).start()

    streams = [(i, owner, p) for i in (1, 0) for owner in (0, 1) for p in range(PARTS)]

    def carry_ring(base):
        def ring_step(step, carry):
            for i, owner, p in streams:
                arrive(base, i, owner, step, 0, p, True)
                arrive(base, i, owner, step, 1, p, step < half - 1)
            return carry

        lax.fori_loop(1, half, ring_step, 0)
        for i, owner, p in streams:
            arrive(base, i, owner, half, 0, p, False)

    def pushed():
        for i in range(2):
            ref = weights.at[RING + which(i), pl.ds(0, wrows * (n_sp - 1))]
            push(ref, ref, i).wait_recv()

    def came_over(base, owner):
        ref = weights.at[base + 2 - parity, pl.ds(0, wrows * (n_sp - 1))]
        over(ref, ref, base, owner).wait_recv()

    def pair_copy(src, dst, send, recv):
        return pltpu.make_async_remote_copy(
            src_ref=src,
            dst_ref=dst,
            send_sem=send,
            recv_sem=recv,
            device_id={"tp": partner},
            device_id_type=MESH,
        )

    def lend(k):
        src, dst = ((gap, gap_there), (shift, shift_there))[k]
        return pair_copy(src, dst, lend_send.at[k], lend_recv.at[k])

    def own_block(m):
        lines = pl.ds(pl.multiple_of(z * wrows, wrows), wrows)
        return pair_copy(
            weights.at[m, lines], others.at[m, lines], own_send.at[m], own_recv.at[m]
        )

    def hand(k):
        src = (vs_there, kf_there, kb_there, rf_there, rb_there)[k]
        dst = (vs, kf, kb, rf, rb)[k]
        return pair_copy(src, dst, hand_send.at[k], hand_recv.at[k])

    @pl.when(carrier)
    def _():
        open_ring(0)
        join_ring(RING)

    @pl.when(jnp.logical_not(carrier))
    def _():
        join_ring(0)
        open_ring(RING)
        for k in range(2):
            lend(k).start()
        for m in range(RING):
            own_block(m).start()

    tok = tokens[...].astype(F32)
    rows = []
    for b in range(seqs):
        part = tok[:, b, :]
        scale = lax.rsqrt(jnp.mean(part * part, axis=-1, keepdims=True) + EPS)
        rows.append(part * scale * gain[...])
    tok_block = pl.ds(pl.multiple_of(here * block_rows, block_rows), block_rows)
    normed[tok_block, :] = jnp.concatenate(rows, axis=0).astype(BF16)

    def token_copy(ref, peer):
        return pltpu.make_async_remote_copy(
            src_ref=ref,
            dst_ref=ref,
            send_sem=tok_send,
            recv_sem=tok_recv,
            device_id={"tp": peer},
            device_id_type=MESH,
        )

    for d in range(1, n_tp):
        token_copy(normed.at[tok_block], lax.rem(tp + d, n_tp)).start()

    @pl.when(carrier)
    def _():
        carry_ring(0)

    rest = normed.at[pl.ds(0, block_rows * (n_tp - 1))]

    def project(matrix):
        return (
            jnp.dot(normed[...], matrix, preferred_element_type=F32).astype(BF16).astype(F32)
        )

    def by_sequence(ref, value):
        for t in range(n_tp):
            for b in range(seqs):
                first = spot(t) * block_rows + b * step_pos
                ref[b, t * step_pos : (t + 1) * step_pos, :] = value[
                    first : first + step_pos, :
                ]

    def silu(u):
        return u / (1.0 + jnp.exp(-u))

    at_row = lax.broadcasted_iota(jnp.int32, (span, span), 0)
    at_col = lax.broadcasted_iota(jnp.int32, (span, span), 1)
    lower = (at_row >= at_col).astype(F32)
    upper = (at_row <= at_col).astype(F32)
    def prepare(matrices, gap_ref, shift_ref, vs_ref, kf_ref, kb_ref, rf_ref, rb_ref, base):
        by_sequence(vs_ref, project(matrices[0]))
        by_sequence(kf_ref, gap_ref[0:1, :] / (1.0 + jnp.exp(project(matrices[1]))))
        by_sequence(kb_ref, gap_ref[1:2, :] / (1.0 + jnp.exp(project(matrices[2]))))
        for b in range(seqs):
            moved = shift_ref[:, b, :]
            fwd_key, bwd_key = kf_ref[b], kb_ref[b]
            fwd_run = jnp.dot(
                lower,
                jnp.log1p(-fwd_key) + moved,
                precision=lax.Precision.HIGHEST,
                preferred_element_type=F32,
            )
            bwd_run = jnp.dot(
                upper,
                jnp.log1p(-bwd_key) + moved,
                precision=lax.Precision.HIGHEST,
                preferred_element_type=F32,
            )
            rf_ref[b] = fwd_run
            rb_ref[b] = bwd_run
            fwd_end, bwd_end = fwd_run[span - 1 : span, :], bwd_run[0:1, :]
            keys = jnp.concatenate(
                [fwd_key * jnp.exp(fwd_end - fwd_run), bwd_key * jnp.exp(bwd_end - bwd_run)],
                axis=1,
            ).astype(BF16)
            states = lax.dot_general(
                vs_ref[b].astype(BF16), keys, dims(((0,), (0,))), preferred_element_type=F32
            )
            for h in range(heads):
                c = b * heads + h
                lanes = slice(h * CH, (h + 1) * CH)
                for d, end in enumerate((fwd_end, bwd_end)):
                    local[d, base + c] = states[
                        lanes, d * width + h * CH : d * width + (h + 1) * CH
                    ].astype(BF16)
                    decay[d, base + c : base + c + 1, :] = jnp.exp(end[:, lanes])

    low_chunks = pl.ds(0, chunks)

    def give_back(d, c):
        return pair_copy(carried.at[d, c], carried.at[d, c - chunks], back_send.at[d], back_recv.at[d])

    def given_back(d):
        ref = carried.at[d, low_chunks]
        return pair_copy(ref, ref, back_send.at[d], back_recv.at[d])

    def ends(d):
        place = (n_sp - 1 - z) if d == 1 else z
        return place // BLK, lax.rem(place, BLK), (-1 if d == 1 else 1)

    def scan_copy(src, dst, send, recv, target):
        return pltpu.make_async_remote_copy(
            src_ref=src,
            dst_ref=dst,
            send_sem=send,
            recv_sem=recv,
            device_id={"sp": target},
            device_id_type=MESH,
        )

    def factor(d, way, j):
        return scan_copy(
            decay.at[d], decay_in.at[d, j - 1], d_send.at[d, j - 1], d_recv.at[d, j - 1], z + j * way
        )

    def near(d, way, c):
        return scan_copy(
            sent1.at[d, c], before.at[d, c], p1_send.at[d], p1_recv.at[d, c], z + way
        )

    def far(d, way, c):
        return scan_copy(
            sent2.at[d, c], ahead.at[d, c], p2_send.at[d, 0], p2_recv.at[d, c], z + BLK * way
        )

    def down(d, way, c):
        return scan_copy(
            sent2.at[d, c], ahead.at[d, c], p2_send.at[d, 1], p2_recv.at[d, c], z + way
        )

    def relay(d, way, c):
        return scan_copy(
            ahead.at[d, c], ahead.at[d, c], p2_send.at[d, 1], p2_recv.at[d, c], z + way
        )

    def clear():
        for d in (0, 1):
            jj, rr, way = ends(d)

            @pl.when(jj == 0)
            def _():
                ahead[d] = jnp.zeros(ahead.shape[1:], ahead.dtype)

            @pl.when(rr == 0)
            def _():
                before[d] = jnp.zeros(before.shape[1:], before.dtype)

    def exchange():
        for d in (0, 1):
            jj, rr, way = ends(d)
            for j in range(1, BLK):

                @pl.when(rr + j < BLK)
                def _():
                    factor(d, way, j).start()

    edge = (lax.rem(z, BLK) == 0) | (lax.rem(z, BLK) == BLK - 1)

    def first_step(d, c):
        jj, rr, way = ends(d)

        @pl.when(rr > 0)
        def _():
            near(d, way, c).wait_recv()

        joined = decay[d, pl.ds(c, 1), :] * before[d, c].astype(F32) + local[d, c].astype(F32)

        @pl.when(rr < BLK - 1)
        def _():
            sent1[d, c] = joined.astype(BF16)
            near(d, way, c).start()

        @pl.when(rr == BLK - 1)
        def _():
            total[d, c] = joined

            @pl.when(jj == 0)
            def _():
                sent2[d, c] = joined.astype(BF16)
                far(d, way, c).start()
                down(d, way, c).start()

    def head_start(d):
        def each(c, carry):
            first_step(d, c)
            return carry

        lax.fori_loop(0, chunks, each, 0)

    def first_pass(d, begin, lag):
        def each(turn, carry):
            @pl.when(turn < 2 * chunks)
            def _():
                first_step(d, turn)

            @pl.when(turn >= lag)
            def _():
                first_step(1 - d, turn - lag)

            return carry

        lax.fori_loop(begin, 2 * chunks + lag, each, 0)

    def factors():
        for d in (0, 1):
            jj, rr, way = ends(d)
            decay_before[d] = jnp.ones(decay_before.shape[1:], F32)
            for j in range(1, BLK):

                @pl.when(rr >= j)
                def _():
                    factor(d, way, j).wait_recv()
                    decay_before[d] = decay_before[d] * decay_in[d, j - 1]

            decay_sent[d] = decay_before[d] * decay[d]

    def second_pass(d):
        jj, rr, way = ends(d)

        def each(c, carry):
            @pl.when(jj > 0)
            def _():
                far(d, way, c).wait_recv()

            @pl.when((rr == BLK - 1) & (jj > 0) & (jj < n_blocks - 1))
            def _():
                joined = (
                    decay_sent[d, pl.ds(c, 1), :] * ahead[d, c].astype(F32) + total[d, c]
                )
                sent2[d, c] = joined.astype(BF16)
                far(d, way, c).start()
                down(d, way, c).start()

            @pl.when((rr < BLK - 2) & (jj > 0))
            def _():
                relay(d, way, c).start()

            carried[d, c] = (
                decay_before[d, pl.ds(c, 1), :] * ahead[d, c].astype(F32)
                + before[d, c].astype(F32)
            ).astype(BF16)

            @pl.when(c >= chunks)
            def _():
                give_back(d, c).start()

            return carry

        lax.fori_loop(0, 2 * chunks, each, 0)

    def inside():
        by_sequence(qs, silu(project(weights[5])))
        by_sequence(gs, silu(project(weights[4])))
        middle = span // 2 - 1
        for b in range(seqs):
            query, fwd_run, bwd_run = qs[b], rf[b], rb[b]
            fwd_mid, bwd_mid = fwd_run[middle : middle + 1, :], bwd_run[middle : middle + 1, :]
            fwd_q = (query * jnp.exp(fwd_run - fwd_mid)).astype(BF16)
            bwd_q = (query * jnp.exp(bwd_run - bwd_mid)).astype(BF16)
            fwd_k = (kf[b] * jnp.exp(fwd_mid - fwd_run)).astype(BF16)
            bwd_k = (kb[b] * jnp.exp(bwd_mid - bwd_run)).astype(BF16)
            fwd_e = (query * jnp.exp(fwd_run)).astype(BF16)
            bwd_e = (query * jnp.exp(bwd_run)).astype(BF16)
            value = vs[b].astype(BF16)
            for h in range(heads):
                c = b * heads + h
                lanes = slice(h * CH, (h + 1) * CH)
                fwd_s = lax.dot_general(
                    fwd_q[:, lanes], fwd_k[:, lanes], dims(((1,), (1,))), preferred_element_type=F32
                )
                bwd_s = lax.dot_general(
                    bwd_q[:, lanes], bwd_k[:, lanes], dims(((1,), (1,))), preferred_element_type=F32
                )
                scores = jnp.where(at_row >= at_col, fwd_s, 0.0) + jnp.where(
                    at_row <= at_col, bwd_s, 0.0
                )
                inner[c] = jnp.dot(
                    scores.astype(BF16), value[:, lanes], preferred_element_type=F32
                )
                qe[c] = jnp.concatenate([fwd_e[:, lanes], bwd_e[:, lanes]], axis=1)

    early = lax.rem(z, BLK) < BLK // 2
    low = z < half

    @pl.when(carrier)
    def _():
        for owner in (0, 1):
            came_over(0, owner)
        clear()
        token_copy(rest, tp).wait_recv()
        prepare([weights[m] for m in range(RING)], gap, shift, vs, kf, kb, rf, rb, 0)

        @pl.when(early & edge)
        def _():
            head_start(0)

        @pl.when(jnp.logical_not(early) & edge)
        def _():
            head_start(1)

        for k in range(2):
            lend(k).wait_recv()
        for m in range(RING):
            own_block(m).wait_recv()
        prepare(
            [others[m] for m in range(RING)],
            gap_there,
            shift_there,
            vs_there,
            kf_there,
            kb_there,
            rf_there,
            rb_there,
            chunks,
        )
        exchange()
        for k in range(5):
            hand(k).start()
        begin = jnp.where(edge, chunks, 0)
        lag = jnp.where(edge, 2 * chunks, LAG)

        @pl.when(early)
        def _():
            first_pass(0, begin, lag)

        @pl.when(jnp.logical_not(early))
        def _():
            first_pass(1, begin, lag)

        factors()

        @pl.when(low)
        def _():
            second_pass(0)

        @pl.when(jnp.logical_not(low))
        def _():
            second_pass(1)

        pushed()

    @pl.when(jnp.logical_not(carrier))
    def _():
        carry_ring(RING)
        token_copy(rest, tp).wait_recv()
        for k in range(5):
            hand(k).wait_recv()

    came_over(RING, 1)
    inside()

    @pl.when(carrier)
    def _():
        @pl.when(low)
        def _():
            second_pass(1)

        @pl.when(jnp.logical_not(low))
        def _():
            second_pass(0)

    @pl.when(jnp.logical_not(carrier))
    def _():
        for d in (0, 1):
            given_back(d).wait_recv()

    for b in range(seqs):
        for h in range(heads):
            c = b * heads + h
            both = inner[c] + lax.dot_general(
                qe[c],
                jnp.concatenate([carried[0, c], carried[1, c]], axis=1),
                dims(((1,), (1,))),
                preferred_element_type=F32,
            )
            scale = lax.rsqrt(jnp.mean(both * both, axis=-1, keepdims=True) + EPS)
            gated = both * scale * head_gain[...] * gs[b, :, h * CH : (h + 1) * CH]
            for t in range(n_tp):
                first = spot(t) * block_rows + b * step_pos
                mixed[first : first + step_pos, h * CH : (h + 1) * CH] = gated[
                    t * step_pos : (t + 1) * step_pos, :
                ]

    side = n_x * block_rows

    def partial(core_index, k):
        lines = pl.ds(pl.multiple_of(core_index * side, side), side)
        return lax.dot_general(
            mixed[lines, :].astype(BF16),
            weights[3, k * (model // STRIPS) : (k + 1) * (model // STRIPS), :],
            dims(((1,), (1,))),
            preferred_element_type=F32,
        )

    strip = model // STRIPS

    def exchange_pair(k):
        columns = pl.ds(k * strip, strip)
        return pair_copy(
            given.at[:, columns], taken.at[:, columns], pair_send.at[k], pair_recv.at[k]
        )

    def piece(dest, d, k):
        lines = pl.ds(pl.multiple_of(dest * block_rows, block_rows), block_rows)
        columns = pl.ds(k * strip, strip)
        return pltpu.make_async_remote_copy(
            src_ref=summed.at[lines, columns],
            dst_ref=pieces.at[d - 1, :, columns],
            send_sem=x_send.at[d - 1, k],
            recv_sem=x_recv.at[d - 1, k],
            device_id={"tp": dest * 2 + core},
            device_id_type=MESH,
        )

    for k in range(STRIPS):
        given[:, k * strip : (k + 1) * strip] = partial(1 - core, k).astype(BF16)
        exchange_pair(k).start()
    for k in range(STRIPS):
        mine[:, k * strip : (k + 1) * strip] = partial(core, k)
    order = [2, 1, 3] if n_x == 4 else list(range(1, n_x))
    for k in range(STRIPS):
        exchange_pair(k).wait_recv()
        columns = slice(k * strip, (k + 1) * strip)
        for d in order:
            dest = lax.rem(x + d, n_x)
            lines = pl.ds(pl.multiple_of(dest * block_rows, block_rows), block_rows)
            summed[lines, columns] = (
                mine[lines, columns] + taken[lines, columns].astype(F32)
            ).astype(BF16)
            piece(dest, d, k).start()
    own_lines = pl.ds(pl.multiple_of(x * block_rows, block_rows), block_rows)
    for k in range(STRIPS):
        columns = slice(k * strip, (k + 1) * strip)
        result = mine[own_lines, columns] + taken[own_lines, columns].astype(F32)
        for d in order:
            piece(x, d, k).wait_recv()
            result = result + pieces[d - 1, :, columns].astype(F32)
        out[:, columns] = result.astype(BF16)

    def ring_left(ref, count, way, i, owner):
        lines = ref.at[0, pl.ds(0, wrows * count)]
        pltpu.make_async_remote_copy(
            src_ref=lines,
            dst_ref=lines,
            send_sem=ring_send.at[way, i, owner],
            recv_sem=ring_recv.at[way, i, owner, 0, 0],
            device_id={"sp": right},
            device_id_type=MESH,
        ).wait_send()

    for i in range(2):
        for way in (0, 1):
            ring_left(weights, half - way, way, i, 0)
            ring_left(weights, half - 1 - way, way, i, 1)
            for p in range(PARTS):
                enter(0, i, way, p).wait_send()
        lines = weights.at[0, pl.ds(0, wrows * (n_sp - 1))]
        over(lines, lines, 0, i).wait_send()
    token_copy(rest, tp).wait_send()
    @pl.when(carrier)
    def _():
        for d in (0, 1):
            jj, rr, way = ends(d)

            @pl.when(rr < BLK - 1)
            def _():
                scan_copy(sent1.at[d], before.at[d], p1_send.at[d], p1_recv.at[d, 0], z).wait_send()

            for j in range(1, BLK):

                @pl.when(rr + j < BLK)
                def _():
                    factor(d, way, j).wait_send()

            leads = (rr == BLK - 1) & (jj < n_blocks - 1)

            @pl.when(leads)
            def _():
                scan_copy(sent2.at[d], ahead.at[d], p2_send.at[d, 0], p2_recv.at[d, 0], z).wait_send()

            @pl.when(leads | ((rr < BLK - 2) & (jj > 0)))
            def _():
                scan_copy(sent2.at[d], ahead.at[d], p2_send.at[d, 1], p2_recv.at[d, 0], z).wait_send()
            given_back(d).wait_send()
        for k in range(5):
            hand(k).wait_send()

    @pl.when(jnp.logical_not(carrier))
    def _():
        for m in range(RING):
            own_block(m).wait_send()
        for k in range(2):
            lend(k).wait_send()
            lines = weights.at[0, pl.ds(0, wrows * (n_sp - 1))]
            push(lines, lines, k).wait_send()

    for k in range(STRIPS):
        exchange_pair(k).wait_send()
        for d in order:
            piece(lax.rem(x + d, n_x), d, k).wait_send()


def shards(
    n_sp,
    n_tp,
    tokens,
    norm_gain,
    w_query,
    w_value,
    w_fwd_gate,
    w_bwd_gate,
    w_out_gate,
    floor_gap,
    decay_shift,
    head_gain,
    w_out,
):
    step_pos, seqs, model = tokens.shape
    wrows, width = w_query.shape
    span = decay_shift.shape[0]
    chunks = seqs * (width // CH)
    both = 2 * chunks
    rows = step_pos * seqs
    all_rows = rows * n_tp
    n_x = n_tp // 2
    f32_rows = pltpu.VMEM((seqs, span, width), F32)
    vmem = pl.BlockSpec(memory_space=pltpu.VMEM)
    dma = pltpu.SemaphoreType.DMA
    result = pl.pallas_call(
        functools.partial(kernel, n_sp, n_tp),
        out_shape=jax.ShapeDtypeStruct((rows, model), BF16),
        in_specs=[vmem] * 11,
        out_specs=vmem,
        scratch_shapes=[
            pltpu.VMEM((6, wrows * n_sp, width), BF16),
            pltpu.VMEM((RING, wrows * n_sp, width), BF16),
            pltpu.VMEM((all_rows, model), BF16),
            pltpu.VMEM((2, width), F32),
            pltpu.VMEM((span, seqs, width), F32),
            f32_rows,
            f32_rows,
            f32_rows,
            f32_rows,
            f32_rows,
            f32_rows,
            f32_rows,
            f32_rows,
            f32_rows,
            f32_rows,
            f32_rows,
            f32_rows,
            pltpu.VMEM((chunks, span, 2 * CH), BF16),
            pltpu.VMEM((chunks, span, CH), F32),
            pltpu.VMEM((2, both, CH, CH), BF16),
            pltpu.VMEM((2, both, CH), F32),
            pltpu.VMEM((2, both, CH, CH), BF16),
            pltpu.VMEM((2, BLK - 1, both, CH), F32),
            pltpu.VMEM((2, both, CH), F32),
            pltpu.VMEM((2, both, CH, CH), BF16),
            pltpu.VMEM((2, both, CH), F32),
            pltpu.VMEM((2, both, CH, CH), F32),
            pltpu.VMEM((2, both, CH, CH), BF16),
            pltpu.VMEM((2, both, CH, CH), BF16),
            pltpu.VMEM((2, both, CH, CH), BF16),
            pltpu.VMEM((all_rows, width), F32),
            pltpu.VMEM((n_x * rows, model), F32),
            pltpu.VMEM((n_x * rows, model), BF16),
            pltpu.VMEM((n_x * rows, model), BF16),
            pltpu.VMEM((n_x * rows, model), BF16),
            pltpu.VMEM((n_x - 1, rows, model), BF16),
            dma((2, 2, 2)),
            dma((2, 2, 2, n_sp // 2 + 1, PARTS)),
            dma((2, 2, PARTS)),
            dma((2,)),
            dma((2,)),
            dma((2,)),
            dma((3,)),
            dma,
            dma,
            dma((2,)),
            dma((2,)),
            dma((RING,)),
            dma((RING,)),
            dma((5,)),
            dma((5,)),
            dma((2,)),
            dma((2,)),
            dma((2, BLK - 1)),
            dma((2, BLK - 1)),
            dma((2,)),
            dma((2, both)),
            dma((2, 2)),
            dma((2, both)),
            dma((STRIPS,)),
            dma((STRIPS,)),
            dma((n_x - 1, STRIPS)),
            dma((n_x - 1, STRIPS)),
        ],
        compiler_params=pltpu.CompilerParams(
            collective_id=0, has_side_effects=True, vmem_limit_bytes=60 * 1024 * 1024
        ),
        name="mixer",
    )(
        tokens,
        norm_gain.reshape(1, -1),
        w_query,
        w_value,
        w_fwd_gate,
        w_bwd_gate,
        w_out_gate,
        w_out.T,
        floor_gap,
        decay_shift,
        head_gain.reshape(1, -1),
    )
    return result.reshape(seqs, step_pos, model).transpose(1, 0, 2)


def solution(mesh):
    in_specs = (
        P(("sp", "tp"), "grp", None),
        P(),
        P("sp", "tp"),
        P("sp", "tp"),
        P("sp", "tp"),
        P("sp", "tp"),
        P("sp", "tp"),
        P(None, "tp"),
        P("sp", "grp", "tp"),
        P(),
        P("tp", "sp"),
    )
    return jax.shard_map(
        functools.partial(shards, mesh.shape["sp"], mesh.shape["tp"]),
        mesh=mesh,
        in_specs=in_specs,
        out_specs=P(("sp", "tp"), "grp", None),
        check_vma=False,
    )
```

time: 321 us -> 173 us (0.54)
  Pallas kernels: 317 us -> 171 us
    pallas_call x1, Pallas kernels: 317 us -> 171 us  [shards(): pl.pallas_call(functools.partial(kernel, n_sp, n_tp), out_shape=jax.Shape...]
where the time goes in v3:
time: 173 us
  Pallas kernels  171 us (99%)
    pallas_call x1, Pallas kernels, shards(): pl.pallas_call(functools.partial(kernel, n_sp, n_tp), out_shape=jax.Shape...  171 us

profile of v3, /device:TPU:97, one launch (start us, length us, event | category | flops | bytes accessed | tf_op | source)
XLA Modules:
  0.0 172.7 jit_solution(3756479343008596184)
XLA Ops:
  0.0 171.1 %mixer.1 = bf16[32,2048]{1,0:T(8,128)(2,1)} custom-call(bf16[8,4,2048]{2,1,0:T(4,128)(2,1)} %tokens.1, f32[1,2048]{1,0:T(1,128)} %bitcast.9, bf16[64,256]{1,0:T(8,128)(2,1)} %w_query.1, bf16[64,256]{1,0:T(8,128)(2,1)} %w_value.1, bf16[64,256]{1,0:T(8,128)(2,1)} %w_fwd.1, bf16[64,256]{1,0:T(8,128)(2,1)} %w_bwd.1, bf16[64,256]{1,0:T(8,128)(2,1)} %w_gate.1, ...), custom_call_target="tpu_custom_call" | custom-call | tf_op jit(solution)/shard_map/mixer/pallas_call | solution.py:817
  171.1 1.7 copy.14

commit v4 on v3

--- a/solution.py
+++ b/solution.py
@@ -27,18 +27,23 @@
 def kernel(
     n_sp,
     n_tp,
-    tokens,
-    gain,
+    tokens_in,
+    gain_in,
     w_query,
     w_value,
     w_fwd,
     w_bwd,
     w_gate,
     w_out,
+    gap_in,
+    shift_in,
+    head_gain_in,
+    out,
+    tokens,
+    gain,
     gap,
     shift,
     head_gain,
-    out,
     weights,
     others,
     normed,
@@ -102,6 +107,7 @@
     pair_recv,
     x_send,
     x_recv,
+    load_sem,
 ):
     z = lax.axis_index("sp")
     tp = lax.axis_index("tp")
@@ -128,8 +134,19 @@
     here = spot(tp)
 
     own_rows = pl.ds(pl.multiple_of(z * wrows, wrows), wrows)
-    for m, ref in enumerate((w_value, w_fwd, w_bwd, w_out, w_gate, w_query)):
-        weights[m, own_rows, :] = ref[...]
+    loads = [
+        (ref, weights.at[m, own_rows])
+        for m, ref in enumerate((w_value, w_fwd, w_bwd, w_out, w_gate, w_query))
+    ] + [
+        (tokens_in, tokens),
+        (gain_in, gain),
+        (gap_in, gap),
+        (shift_in, shift),
+        (head_gain_in, head_gain),
+    ]
+    loads = [
+        pltpu.make_async_copy(src, dst, load_sem.at[k]) for k, (src, dst) in enumerate(loads)
+    ]
 
     barrier = pltpu.get_barrier_semaphore()
     greeted = 0
@@ -140,7 +157,11 @@
     ):
         pl.semaphore_signal(barrier, inc=1, device_id=peer, device_id_type=MESH)
         greeted += 1
+    for load in loads:
+        load.start()
     pl.semaphore_wait(barrier, greeted)
+    for load in loads[:6]:
+        load.wait()
 
     share = wrows // PARTS
 
@@ -282,10 +303,16 @@
     def _():
         join_ring(0)
         open_ring(RING)
+        for m in range(RING):
+            own_block(m).start()
+
+    for load in loads[6:]:
+        load.wait()
+
+    @pl.when(jnp.logical_not(carrier))
+    def _():
         for k in range(2):
             lend(k).start()
-        for m in range(RING):
-            own_block(m).start()
 
     tok = tokens[...].astype(F32)
     rows = []
@@ -317,7 +344,7 @@
 
     def project(matrix):
         return (
-            jnp.dot(normed[...], matrix, preferred_element_type=F32).astype(BF16).astype(F32)
+            jnp.dot(normed[...], matrix[...], preferred_element_type=F32).astype(BF16).astype(F32)
         )
 
     def by_sequence(ref, value):
@@ -337,8 +364,20 @@
     upper = (at_row <= at_col).astype(F32)
     def prepare(matrices, gap_ref, shift_ref, vs_ref, kf_ref, kb_ref, rf_ref, rb_ref, base):
         by_sequence(vs_ref, project(matrices[0]))
-        by_sequence(kf_ref, gap_ref[0:1, :] / (1.0 + jnp.exp(project(matrices[1]))))
-        by_sequence(kb_ref, gap_ref[1:2, :] / (1.0 + jnp.exp(project(matrices[2]))))
+
+        def keys_of(d):
+            key = gap_ref[d : d + 1, :] / (1.0 + jnp.exp(project(matrices[1 + d])))
+            by_sequence((kf_ref, kb_ref)[d], key)
+
+        for first in (True, False):
+            if not first:
+                came_over(0, 1 if base else 0)
+            for d in (0, 1):
+
+                @pl.when(parity == (d if first else 1 - d))
+                def _():
+                    keys_of(d)
+
         for b in range(seqs):
             moved = shift_ref[:, b, :]
             fwd_key, bwd_key = kf_ref[b], kb_ref[b]
@@ -537,8 +576,8 @@
         lax.fori_loop(0, 2 * chunks, each, 0)
 
     def inside():
-        by_sequence(qs, silu(project(weights[5])))
-        by_sequence(gs, silu(project(weights[4])))
+        by_sequence(qs, silu(project(weights.at[5])))
+        by_sequence(gs, silu(project(weights.at[4])))
         middle = span // 2 - 1
         for b in range(seqs):
             query, fwd_run, bwd_run = qs[b], rf[b], rb[b]
@@ -572,11 +611,9 @@
 
     @pl.when(carrier)
     def _():
-        for owner in (0, 1):
-            came_over(0, owner)
         clear()
         token_copy(rest, tp).wait_recv()
-        prepare([weights[m] for m in range(RING)], gap, shift, vs, kf, kb, rf, rb, 0)
+        prepare([weights.at[m] for m in range(RING)], gap, shift, vs, kf, kb, rf, rb, 0)
 
         @pl.when(early & edge)
         def _():
@@ -591,7 +628,7 @@
         for m in range(RING):
             own_block(m).wait_recv()
         prepare(
-            [others[m] for m in range(RING)],
+            [others.at[m] for m in range(RING)],
             gap_there,
             shift_there,
             vs_there,
@@ -817,9 +854,14 @@
     result = pl.pallas_call(
         functools.partial(kernel, n_sp, n_tp),
         out_shape=jax.ShapeDtypeStruct((rows, model), BF16),
-        in_specs=[vmem] * 11,
+        in_specs=[pl.BlockSpec(memory_space=pl.ANY)] * 11,
         out_specs=vmem,
         scratch_shapes=[
+            pltpu.VMEM(tokens.shape, BF16),
+            pltpu.VMEM((1, model), F32),
+            pltpu.VMEM((2, width), F32),
+            pltpu.VMEM((span, seqs, width), F32),
+            pltpu.VMEM((1, CH), F32),
             pltpu.VMEM((6, wrows * n_sp, width), BF16),
             pltpu.VMEM((RING, wrows * n_sp, width), BF16),
             pltpu.VMEM((all_rows, model), BF16),
@@ -883,6 +925,7 @@
             dma((STRIPS,)),
             dma((n_x - 1, STRIPS)),
             dma((n_x - 1, STRIPS)),
+            dma((11,)),
         ],
         compiler_params=pltpu.CompilerParams(
             collective_id=0, has_side_effects=True, vmem_limit_bytes=60 * 1024 * 1024

time: 173 us -> 171 us (0.988)
  no operation moved by 1% of the time
where the time goes in v4:
time: 171 us
  Pallas kernels  170 us (99%)
    pallas_call x1, Pallas kernels, shards(): pl.pallas_call(functools.partial(kernel, n_sp, n_tp), out_shape=jax.Shape...  170 us

profile of v4, /device:TPU:97, one launch (start us, length us, event | category | flops | bytes accessed | tf_op | source)
XLA Modules:
  0.0 171.3 jit_solution(3735281145647406356)
XLA Ops:
  0.0 169.6 %mixer.1 = bf16[32,2048]{1,0:T(8,128)(2,1)} custom-call(bf16[8,4,2048]{2,1,0:T(4,128)(2,1)} %tokens_in.1, f32[1,2048]{1,0:T(1,128)} %bitcast.9, bf16[64,256]{1,0:T(8,128)(2,1)} %w_query.1, bf16[64,256]{1,0:T(8,128)(2,1)} %w_value.1, bf16[64,256]{1,0:T(8,128)(2,1)} %w_fwd.1, bf16[64,256]{1,0:T(8,128)(2,1)} %w_bwd.1, bf16[64,256]{1,0:T(8,128)(2,1)} %w_gate.1, ...), custom_call_target="tpu_custom_call" | custom-call | tf_op jit(solution)/shard_map/mixer/pallas_call | solution.py:854
  169.6 1.7 copy.14

commit v5 on v4

--- a/solution.py
+++ b/solution.py
@@ -607,7 +607,10 @@
                 qe[c] = jnp.concatenate([fwd_e[:, lanes], bwd_e[:, lanes]], axis=1)
 
     early = lax.rem(z, BLK) < BLK // 2
-    low = z < half
+    near_end = jnp.where(z < half, z, n_sp - 1 - z)
+    waits = near_end // BLK > 0
+    leads_other = (near_end // BLK == n_blocks // 2 - 1) & (lax.rem(near_end, BLK) == 0)
+    low = (z < half) != leads_other
 
     @pl.when(carrier)
     def _():
@@ -654,6 +657,15 @@
 
         factors()
 
+        def own_part():
+            pushed()
+            came_over(RING, 1)
+            inside()
+
+        @pl.when(waits)
+        def _():
+            own_part()
+
         @pl.when(low)
         def _():
             second_pass(0)
@@ -662,7 +674,9 @@
         def _():
             second_pass(1)
 
-        pushed()
+        @pl.when(jnp.logical_not(waits))
+        def _():
+            own_part()
 
     @pl.when(jnp.logical_not(carrier))
     def _():
@@ -670,9 +684,8 @@
         token_copy(rest, tp).wait_recv()
         for k in range(5):
             hand(k).wait_recv()
-
-    came_over(RING, 1)
-    inside()
+        came_over(RING, 1)
+        inside()
 
     @pl.when(carrier)
     def _():

time: 171 us -> 164 us (0.959)
  Pallas kernels: 170 us -> 163 us
    pallas_call x1, Pallas kernels: 170 us -> 163 us  [shards(): pl.pallas_call(functools.partial(kernel, n_sp, n_tp), out_shape=jax.Shape...]
where the time goes in v5:
time: 164 us
  Pallas kernels  163 us (99%)
  local copies, waits for them, and re-layouts  1.66 us (1%)
    pallas_call x1, Pallas kernels, shards(): pl.pallas_call(functools.partial(kernel, n_sp, n_tp), out_shape=jax.Shape...  163 us

profile of v5, /device:TPU:97, one launch (start us, length us, event | category | flops | bytes accessed | tf_op | source)
XLA Modules:
  0.0 164.3 jit_solution(9777497420818627039)
XLA Ops:
  0.0 162.6 %mixer.1 = bf16[32,2048]{1,0:T(8,128)(2,1)} custom-call(bf16[8,4,2048]{2,1,0:T(4,128)(2,1)} %tokens_in.1, f32[1,2048]{1,0:T(1,128)} %bitcast.9, bf16[64,256]{1,0:T(8,128)(2,1)} %w_query.1, bf16[64,256]{1,0:T(8,128)(2,1)} %w_value.1, bf16[64,256]{1,0:T(8,128)(2,1)} %w_fwd.1, bf16[64,256]{1,0:T(8,128)(2,1)} %w_bwd.1, bf16[64,256]{1,0:T(8,128)(2,1)} %w_gate.1, ...), custom_call_target="tpu_custom_call" | custom-call | tf_op jit(solution)/shard_map/mixer/pallas_call | solution.py:867
  162.6 1.7 %copy.14 = bf16[4,8,2048]{2,0,1:T(4,128)(2,1)} copy(bf16[4,8,2048]{2,1,0:T(8,128)(2,1)} %bitcast.7) | data formatting | bytes 262144 | tf_op jit(solution)/shard_map/reshape | solution.py:960
